TPU v7x, 32 devices: a whole 2x2x4 slice. The times are simulated.
32 devices in a mesh: grp: 2 (over y), sp: 4 (over z), dp: 4 (over x, core).
Axes of the slice: x: 2, y: 2, z: 4, core: 2. Of those that a mesh axis runs over, the one named last changes fastest.
Arguments:
- gate_input: bfloat16 [8, 1536, 2048], P(('grp', 'dp'), 'sp'), parts along dimension 0, may hold values from -6 to 6
- value_input: bfloat16 [8, 1536, 2048], P(('grp', 'dp'), 'sp'), parts along dimension 0, may hold values from -6 to 6
- norm_gain: bfloat16 [2048], replicated, may hold values from 0.099609375 to 1.8984375
- norm_bias: bfloat16 [2048], replicated, may hold values from -2.5 to 2.5
- mix_weight: bfloat16 [16, 1024, 1024], P('sp', 'dp'), may hold values from -0.1875 to 0.1875
- mix_bias: bfloat16 [16, 1024], P('sp'), may hold values from 0.099609375 to 1.8984375
Outputs:
- gated: bfloat16 [8, 1536, 2048], P(('grp', 'dp'), 'sp'), parts along dimension 0
There are 2 independent parts, one for each index of `grp`. A program takes and returns all parts, laid end to end along the dimension named above; an argument that names none is the same for every part. Nothing has to cross between parts.
All inputs are finite; a program needn't handle non-finite values.
Results may differ from a plain program's by a relative error of at most 0.0053.
Values may be sent and summed in bfloat16 or wider, within the bound.
A program may use at most 64 MiB of HBM per device.

v0:
```python
import jax
import jax.numpy as jnp
from jax import lax
from jax.sharding import PartitionSpec as P

GD = 128
BLK = 1024


def mix_groups(normed_ex, mix_weight, mix_bias):
    seqs, length, local_width = normed_ex.shape
    groups_here = mix_weight.shape[0]
    nblocks = -(-length // BLK)
    padded = jnp.pad(normed_ex, ((0, 0), (0, nblocks * BLK - length), (0, 0)))
    blocks = padded.reshape(seqs * nblocks, BLK, groups_here, GD)
    piece = lax.all_gather(mix_weight, "dp", axis=1, tiled=True)
    count = piece.shape[1]
    rows = lax.iota(jnp.int32, count)
    cols = lax.iota(jnp.int32, BLK)
    keep = cols[None, :] <= rows[:, None]
    masked = jnp.where(keep[None], piece, jnp.zeros_like(piece))
    term = jnp.einsum("gts,bsgc->btgc", masked, blocks, preferred_element_type=jnp.float32)
    bias_rows = mix_bias.astype(jnp.float32)
    mixed = term + bias_rows.T[None, :, :, None]
    mixed = mixed.reshape(seqs, nblocks * BLK, local_width)[:, :length]
    return mixed.astype(jnp.bfloat16)


def body(gate_input, value_input, norm_gain, norm_bias, mix_weight, mix_bias):
    act = jax.nn.gelu(value_input.astype(jnp.float32))
    mean = jnp.mean(act, axis=-1, keepdims=True)
    var = jnp.mean(jnp.square(act - mean), axis=-1, keepdims=True)
    normed = (
        (act - mean) * lax.rsqrt(var + 1e-06) * norm_gain.astype(jnp.float32)
        + norm_bias.astype(jnp.float32)
    ).astype(jnp.bfloat16)
    normed_ex = lax.all_to_all(normed, "sp", split_axis=2, concat_axis=1, tiled=True)
    mixed = mix_groups(normed_ex, mix_weight, mix_bias)
    returned = lax.all_to_all(mixed, "sp", split_axis=1, concat_axis=2, tiled=True)
    gated = jax.nn.gelu(gate_input.astype(jnp.float32)) * returned.astype(jnp.float32)
    return gated.astype(jnp.bfloat16)


def solution(mesh):
    placed = (
        P(("grp", "dp"), "sp", None),
        P(("grp", "dp"), "sp", None),
        P(),
        P(),
        P("sp", "dp", None),
        P("sp", None),
    )
    return jax.shard_map(
        body, mesh=mesh, in_specs=placed, out_specs=P(("grp", "dp"), "sp", None), check_vma=False
    )
```

profile of v0, /device:TPU:0, one launch (start us, length us, event | category | flops | bytes accessed | tf_op | source)
XLA Modules:
  0.0 239.9 jit_solution(9603832664579578522)
XLA Ops:
  6.5 0.0 copy-start
  6.5 0.0 copy-start.4
  6.5 0.0 copy-start.5
  6.5 0.0 all-gather.2.cloned.1.call-start
  6.5 0.7 all-gather.2.cloned.1.call-update
  7.3 0.7 copy-done
  7.9 0.9 copy.17
  8.8 0.0 copy-done.4
  8.8 0.0 copy-done.5
  8.8 1.1 fusion.23
  10.0 1.3 multiply_reduce_fusion
  11.3 1.5 add_convert_fusion
  12.9 30.1 %copy.35 = bf16[1,384,2048]{1,0,2:T(2,128)(2,1)S(1)} copy(bf16[1,384,2048]{1,2,0:T(8,128)(2,1)S(1)} %add_convert_fusion) | data formatting | bytes 3145728 | tf_op jit(solution)/shard_map/convert_element_type | solution.py:36
  43.0 0.5 broadcast.85
  43.5 34.4 %reduce.2 = bf16[2048,384]{1,0:T(8,128)(2,1)} reduce(bf16[2048,1,384]{2,1,0:T(2,128)(2,1)S(1)} %bitcast.31, bf16[]{:T(256)} %broadcast.85), dimensions={1}, to_apply=%bitcast.30.reduce_sub_computation | reduce | bytes 3145730
  77.9 0.0 copy-start.3
  77.9 3.7 %reshape.69 = bf16[4,2,98304]{2,1,0:T(2,128)(2,1)} reshape(bf16[2048,384]{1,0:T(8,128)(2,1)} %reduce.2) | data formatting | bytes 3145728
  81.7 6.3 %all-to-all-start = ((bf16[4,2,98304]{2,1,0:T(2,128)(2,1)}), bf16[4,2,98304]{2,1,0:T(2,128)(2,1)}, u32[]{:S(2)}, u32[]{:S(2)}) async-start(bf16[4,2,98304]{2,1,0:T(2,128)(2,1)} %reshape.69), calls=%async_computation | async-start | bytes 3145728 | tf_op jit(solution)/shard_map/all_to_all | solution.py:37
  88.0 1.3 iota_compare_fusion
  89.3 0.0 copy-done.3
  89.3 35.8 %all-to-all-done = bf16[4,2,98304]{2,1,0:T(2,128)(2,1)} async-done(((bf16[4,2,98304]{2,1,0:T(2,128)(2,1)}), bf16[4,2,98304]{2,1,0:T(2,128)(2,1)}, u32[]{:S(2)}, u32[]{:S(2)}) %all-to-all-start) | async-done | bytes 1572896 | tf_op jit(solution)/shard_map/all_to_all | solution.py:37
  125.1 3.1 %reshape.70 = bf16[2048,1,384]{2,1,0:T(2,128)(2,1)S(1)} reshape(bf16[4,2,98304]{2,1,0:T(2,128)(2,1)} %all-to-all-done) | data formatting | bytes 3145728
  128.2 1.4 copy.27
  129.6 2.6 %copy.19 = bf16[1,4,384,512]{3,2,1,0:T(8,128)(2,1)} copy(bf16[1,4,384,512]{2,3,1,0:T(8,128)(2,1)} %bitcast.36) | data formatting | bytes 3145728 | tf_op jit(solution)/shard_map/all_to_all | solution.py:37
  132.2 0.0 copy-start.2
  132.2 1.6 pad.4
  133.8 2.1 reshape.64
  135.9 0.0 all-gather.2.cloned.1.call-done
  135.9 0.0 copy-done.2
  135.9 8.1 %fusion.4 = bf16[2,1024,4,128]{1,3,0,2:T(8,128)(2,1)} fusion(f32[1024,4]{0,1:T(4,128)S(1)} %convert_bitcast_fusion.1, bf16[4,1024,1024]{2,1,0:T(8,128)(2,1)} %all-gather.2.cloned.1.call-done, pred[1024,1024]{1,0:T(8,128)(4,1)S(1)} %copy-done.2, bf16[2,1024,4,128]{3,2,1,0:T(4,128)(2,1)} %reshape.64), kind=kOutput, calls=%fused_computation.13 | convolution fusion | flops 2153775104 | bytes 13647872 | tf_op jit(solution)/shard_map/gts,bsgc->btgc/dot_general | solution.py:22
  144.0 3.1 %copy.21 = bf16[2,1024,4,128]{3,2,1,0:T(4,128)(2,1)S(1)} copy(bf16[2,1024,4,128]{1,3,0,2:T(8,128)(2,1)} %fusion.4) | data formatting | bytes 4194304 | tf_op jit(solution)/shard_map/convert.5
  147.2 2.2 reshape.65
  149.4 0.0 slice-start
  149.4 1.4 slice-done
  150.8 11.7 %copy.34 = bf16[1,1536,512]{2,0,1:T(2,128)(2,1)S(1)} copy(bf16[1,1536,512]{2,1,0:T(8,128)(2,1)S(1)} %slice-done) | data formatting | bytes 3145728 | tf_op jit(solution)/shard_map/slice | solution.py:25
  162.5 11.1 %reduce.3 = bf16[1536,512]{1,0:T(8,128)(2,1)} reduce(bf16[1536,1,512]{2,1,0:T(2,128)(2,1)S(1)} %bitcast.32, bf16[]{:T(256)} %broadcast.85), dimensions={1}, to_apply=%bitcast.29.reduce_sub_computation | reduce | bytes 3145730
  173.5 0.0 copy-start.1
  173.5 4.3 %reshape.71 = bf16[4,2,98304]{2,1,0:T(2,128)(2,1)} reshape(bf16[1536,512]{1,0:T(8,128)(2,1)} %reduce.3) | data formatting | bytes 3145728
  177.8 4.3 %all-to-all-start.1 = ((bf16[4,2,98304]{2,1,0:T(2,128)(2,1)}), bf16[4,2,98304]{2,1,0:T(2,128)(2,1)}, u32[]{:S(2)}, u32[]{:S(2)}) async-start(bf16[4,2,98304]{2,1,0:T(2,128)(2,1)} %reshape.71), calls=%async_computation.1 | async-start | bytes 3145728 | tf_op jit(solution)/shard_map/all_to_all | solution.py:39
  182.1 0.0 copy-done.1
  182.2 1.6 copy.16
  183.7 35.0 %all-to-all-done.1 = bf16[4,2,98304]{2,1,0:T(2,128)(2,1)} async-done(((bf16[4,2,98304]{2,1,0:T(2,128)(2,1)}), bf16[4,2,98304]{2,1,0:T(2,128)(2,1)}, u32[]{:S(2)}, u32[]{:S(2)}) %all-to-all-start.1) | async-done | bytes 1572896 | tf_op jit(solution)/shard_map/all_to_all | solution.py:39
  218.7 3.1 %reshape.72 = bf16[1536,1,512]{2,1,0:T(2,128)(2,1)S(1)} reshape(bf16[4,2,98304]{2,1,0:T(2,128)(2,1)} %all-to-all-done.1) | data formatting | bytes 3145728
  221.8 0.4 copy.23
  222.2 2.1 convert_bitcast_fusion
  224.3 2.4 copy.24
  226.7 3.8 %fusion.12 = bf16[1,384,2048]{1,2,0:T(8,128)(2,1)} fusion(bf16[1,384,2048]{1,2,0:T(8,128)(2,1)} %copy.16, f32[1,384,4,512]{1,3,2,0:T(8,128)S(1)} %copy.24), kind=kLoop, calls=%fused_computation.22 | loop fusion | flops 8650752 | bytes 6291456 | tf_op jit(solution)/shard_map/convert_element_type | solution.py:41
  230.5 2.6 %copy.25 = bf16[1,384,2048]{2,1,0:T(8,128)(2,1)} copy(bf16[1,384,2048]{1,2,0:T(8,128)(2,1)} %fusion.12) | data formatting | bytes 3145728 | tf_op jit(solution)/shard_map/convert_element_type | solution.py:41
  (5 shorter events, 0.0 us)
Async XLA Ops:
  6.5 1.4 copy-start
  6.5 2.3 copy-start.4
  6.5 2.3 copy-start.5
  6.5 129.4 %all-gather.2.cloned.1.call-start = ((), (), s32[]{:S(2)}) async-start(), calls=%async_computation.2 | async-start | bytes 10485760 | tf_op jit(solution)/shard_map/all_gather | solution.py:16
  77.9 11.4 %copy-start.3 = (bf16[4,1024]{1,0:T(4,128)(2,1)S(1)}, bf16[4,1024]{1,0:T(4,128)(2,1)}, u32[]{:S(2)}) copy-start(bf16[4,1024]{1,0:T(4,128)(2,1)} %param.11) | copy-start | bytes 24580
  81.7 43.4 %all-to-all-start = ((bf16[4,2,98304]{2,1,0:T(2,128)(2,1)}), bf16[4,2,98304]{2,1,0:T(2,128)(2,1)}, u32[]{:S(2)}, u32[]{:S(2)}) async-start(bf16[4,2,98304]{2,1,0:T(2,128)(2,1)} %reshape.69), calls=%async_computation | async-start | bytes 3145728 | tf_op jit(solution)/shard_map/all_to_all | solution.py:37
  132.2 3.7 %copy-start.2 = (pred[1024,1024]{1,0:T(8,128)(4,1)S(1)}, pred[1024,1024]{1,0:T(8,128)(4,1)}, u32[]{:S(2)}) copy-start(pred[1024,1024]{1,0:T(8,128)(4,1)} %iota_compare_fusion) | copy-start | bytes 3145732
  149.4 1.4 slice-start
  173.5 8.6 %copy-start.1 = (bf16[1,384,2048]{2,1,0:T(8,128)(2,1)S(1)}, bf16[1,384,2048]{2,1,0:T(8,128)(2,1)}, u32[]{:S(2)}) copy-start(bf16[1,384,2048]{2,1,0:T(8,128)(2,1)} %param.6) | copy-start | bytes 4718596
  177.8 40.9 %all-to-all-start.1 = ((bf16[4,2,98304]{2,1,0:T(2,128)(2,1)}), bf16[4,2,98304]{2,1,0:T(2,128)(2,1)}, u32[]{:S(2)}, u32[]{:S(2)}) async-start(bf16[4,2,98304]{2,1,0:T(2,128)(2,1)} %reshape.71), calls=%async_computation.1 | async-start | bytes 3145728 | tf_op jit(solution)/shard_map/all_to_all | solution.py:39
Sparse Core Ops, SparseCore 0:
  8.9 60.9 all-gather.1
where the time goes:
time: 241 us; the launch traced here: 240 us
  local copies, waits for them, and re-layouts  79.4 us (33%)
  waiting for transfers between devices  71.5 us (30%)
  other arithmetic  56.7 us (24%)
  between operations  13.5 us (6%)
  starting transfers between devices  10.7 us (4%)
  matrix products  8.09 us (3%)
    unnamed x2, other arithmetic  45.5 us
    all_to_all x1, waiting for transfers between devices, body(): lax.all_to_all(normed, 'sp', split_axis=2, concat_axis=1, tiled=True)  35.8 us
    all_to_all x1, waiting for transfers between devices, body(): lax.all_to_all(mixed, 'sp', split_axis=1, concat_axis=2, tiled=True)  35 us
    convert_element_type x1, local copies, waits for them, and re-layouts, body(): normed = ((act - mean) * lax.rsqrt(var + 1e-06) * norm_gain.astype(jnp.fl...  30.1 us
    unnamed x20, local copies, waits for them, and re-layouts  19.2 us
    slice x3, local copies, waits for them, and re-layouts, mix_groups(): mixed = mixed.reshape(seqs, nblocks * BLK, local_width)[:, :length]  13.1 us
    dot_general x1, matrix products, mix_groups(): jnp.einsum('gts,bsgc->btgc', masked, blocks, preferred_element_type=jnp.f...  8.09 us
    all_to_all x1, starting transfers between devices, body(): lax.all_to_all(normed, 'sp', split_axis=2, concat_axis=1, tiled=True)  6.35 us
  transfers between devices with their start and end apart: 3, of which 2 were waited for; matrix products, arithmetic and copies ran while one was open for 36% of the time, Pallas kernels for 0%

commit v1 on v0

--- a/solution.py
+++ b/solution.py
@@ -36,7 +36,9 @@
     ).astype(jnp.bfloat16)
     normed_ex = lax.all_to_all(normed, "sp", split_axis=2, concat_axis=1, tiled=True)
     mixed = mix_groups(normed_ex, mix_weight, mix_bias)
-    returned = lax.all_to_all(mixed, "sp", split_axis=1, concat_axis=2, tiled=True)
+    returned = jnp.concatenate(
+        lax.all_to_all(jnp.stack(jnp.split(mixed, lax.axis_size("sp"), axis=1)), "sp", 0, 0), axis=2
+    )
     gated = jax.nn.gelu(gate_input.astype(jnp.float32)) * returned.astype(jnp.float32)
     return gated.astype(jnp.bfloat16)
 

time: 241 us -> 211 us (0.88)
  local copies, waits for them, and re-layouts: 79.4 us -> 60.1 us
  other arithmetic: 56.7 us -> 47 us
    slice x3 -> x0, local copies, waits for them, and re-layouts: 13.1 us -> none  [mix_groups(): mixed = mixed.reshape(seqs, nblocks * BLK, local_width)[:, :length]]
    unnamed x2 -> x1, other arithmetic: 45.5 us -> 34.4 us
    unnamed x20 -> x18, local copies, waits for them, and re-layouts: 19.2 us -> 11.9 us
  transfers between devices with their start and end apart: 3 -> 3, of which waited for: 2 -> 2; matrix products, arithmetic and copies ran while one was open for 36% -> 42% of each run, Pallas kernels for 0% -> 0%
where the time goes in v1:
time: 211 us; the launch traced here: 210 us
  waiting for transfers between devices  71.4 us (34%)
  local copies, waits for them, and re-layouts  60.1 us (28%)
  other arithmetic  47 us (22%)
  between operations  13.5 us (6%)
  starting transfers between devices  9.91 us (5%)
  matrix products  8.1 us (4%)
    all_to_all x1, waiting for transfers between devices, body(): lax.all_to_all(normed, 'sp', split_axis=2, concat_axis=1, tiled=True)  35.8 us
    all_to_all x1, waiting for transfers between devices, body(): lax.all_to_all(jnp.stack(jnp.split(mixed, lax.axis_size('sp'), axis=1)),...  34.9 us
    unnamed x1, other arithmetic  34.4 us
    convert_element_type x1, local copies, waits for them, and re-layouts, body(): normed = ((act - mean) * lax.rsqrt(var + 1e-06) * norm_gain.astype(jnp.fl...  30.1 us
    unnamed x18, local copies, waits for them, and re-layouts  11.9 us
    dot_general x1, matrix products, mix_groups(): jnp.einsum('gts,bsgc->btgc', masked, blocks, preferred_element_type=jnp.f...  8.1 us
    all_to_all x1, starting transfers between devices, body(): lax.all_to_all(normed, 'sp', split_axis=2, concat_axis=1, tiled=True)  6.35 us
  transfers between devices with their start and end apart: 3, of which 2 were waited for; matrix products, arithmetic and copies ran while one was open for 42% of the time, Pallas kernels for 0%

profile of v1, /device:TPU:0, one launch (start us, length us, event | category | flops | bytes accessed | tf_op | source)
XLA Modules:
  0.0 209.9 jit_solution(4532512922358735839)
XLA Ops:
  6.5 0.0 copy-start
  6.5 0.0 copy-start.4
  6.5 0.0 copy-start.5
  6.5 0.0 all-gather.2.cloned.1.call-start
  6.5 0.7 all-gather.2.cloned.1.call-update
  7.3 0.7 copy-done
  7.9 0.9 copy.20
  8.8 0.0 copy-done.4
  8.8 0.0 copy-done.5
  8.8 1.1 fusion.23
  10.0 1.3 multiply_reduce_fusion
  11.3 1.5 add_convert_fusion
  12.9 30.1 %copy.34 = bf16[1,384,2048]{1,0,2:T(2,128)(2,1)S(1)} copy(bf16[1,384,2048]{1,2,0:T(8,128)(2,1)S(1)} %add_convert_fusion) | data formatting | bytes 3145728 | tf_op jit(solution)/shard_map/convert_element_type | solution.py:36
  43.0 0.6 broadcast.85
  43.6 34.4 %reduce.2 = bf16[2048,384]{1,0:T(8,128)(2,1)} reduce(bf16[2048,1,384]{2,1,0:T(2,128)(2,1)S(1)} %bitcast.33, bf16[]{:T(256)} %broadcast.85), dimensions={1}, to_apply=%bitcast.32.reduce_sub_computation | reduce | bytes 3145730
  78.0 0.0 copy-start.3
  78.0 3.7 %reshape.68 = bf16[4,2,98304]{2,1,0:T(2,128)(2,1)} reshape(bf16[2048,384]{1,0:T(8,128)(2,1)} %reduce.2) | data formatting | bytes 3145728
  81.7 6.3 %all-to-all-start = ((bf16[4,2,98304]{2,1,0:T(2,128)(2,1)}), bf16[4,2,98304]{2,1,0:T(2,128)(2,1)}, u32[]{:S(2)}, u32[]{:S(2)}) async-start(bf16[4,2,98304]{2,1,0:T(2,128)(2,1)} %reshape.68), calls=%async_computation | async-start | bytes 3145728 | tf_op jit(solution)/shard_map/all_to_all | solution.py:37
  88.0 1.3 iota_compare_fusion
  89.3 0.0 copy-done.3
  89.4 35.8 %all-to-all-done = bf16[4,2,98304]{2,1,0:T(2,128)(2,1)} async-done(((bf16[4,2,98304]{2,1,0:T(2,128)(2,1)}), bf16[4,2,98304]{2,1,0:T(2,128)(2,1)}, u32[]{:S(2)}, u32[]{:S(2)}) %all-to-all-start) | async-done | bytes 1572896 | tf_op jit(solution)/shard_map/all_to_all | solution.py:37
  125.1 3.1 %reshape.69 = bf16[2048,1,384]{2,1,0:T(2,128)(2,1)S(1)} reshape(bf16[4,2,98304]{2,1,0:T(2,128)(2,1)} %all-to-all-done) | data formatting | bytes 3145728
  128.2 1.4 copy.28
  129.6 2.6 %copy.22 = bf16[1,4,384,512]{3,2,1,0:T(8,128)(2,1)} copy(bf16[1,4,384,512]{2,3,1,0:T(8,128)(2,1)} %bitcast.36) | data formatting | bytes 3145728 | tf_op jit(solution)/shard_map/all_to_all | solution.py:37
  132.2 0.0 copy-start.2
  132.2 1.6 pad.4
  133.8 2.1 reshape.64
  135.9 0.0 all-gather.2.cloned.1.call-done
  135.9 0.0 copy-done.2
  135.9 8.1 %fusion.4 = bf16[2,1024,4,128]{1,3,0,2:T(8,128)(2,1)} fusion(f32[1024,4]{0,1:T(4,128)S(1)} %convert_bitcast_fusion.1, bf16[4,1024,1024]{2,1,0:T(8,128)(2,1)} %all-gather.2.cloned.1.call-done, pred[1024,1024]{1,0:T(8,128)(4,1)S(1)} %copy-done.2, bf16[2,1024,4,128]{3,2,1,0:T(4,128)(2,1)} %reshape.64), kind=kOutput, calls=%fused_computation.13 | convolution fusion | flops 2153775104 | bytes 13647872 | tf_op jit(solution)/shard_map/gts,bsgc->btgc/dot_general | solution.py:22
  144.0 3.1 %copy.24 = bf16[2,1024,4,128]{3,2,1,0:T(4,128)(2,1)S(1)} copy(bf16[2,1024,4,128]{1,3,0,2:T(8,128)(2,1)} %fusion.4) | data formatting | bytes 4194304 | tf_op jit(solution)/shard_map/convert.4
  147.2 2.2 %reshape.65 = bf16[1,2048,512]{2,1,0:T(8,128)(2,1)} reshape(bf16[2,1024,4,128]{3,2,1,0:T(4,128)(2,1)S(1)} %copy.24) | data formatting | bytes 4194304 | tf_op jit(solution)/shard_map/reshape | solution.py:25
  149.4 1.5 slice_bitcast_fusion.3
  150.8 0.0 copy-start.1
  150.9 1.4 pad_maximum_fusion
  152.2 3.6 %all-to-all-start.1 = ((bf16[4,1,384,512]{3,2,1,0:T(8,128)(2,1)}), bf16[4,1,384,512]{3,2,1,0:T(8,128)(2,1)S(1)}, u32[]{:S(2)}, u32[]{:S(2)}) async-start(bf16[4,1,384,512]{3,2,1,0:T(8,128)(2,1)} %pad_maximum_fusion), calls=%async_computation.1 | async-start | bytes 3145728 | tf_op jit(solution)/shard_map/all_to_all | solution.py:40
  155.8 0.0 copy-done.1
  155.8 1.6 copy.19
  157.4 34.9 %all-to-all-done.1 = bf16[4,1,384,512]{3,2,1,0:T(8,128)(2,1)S(1)} async-done(((bf16[4,1,384,512]{3,2,1,0:T(8,128)(2,1)}), bf16[4,1,384,512]{3,2,1,0:T(8,128)(2,1)S(1)}, u32[]{:S(2)}, u32[]{:S(2)}) %all-to-all-start.1) | async-done | bytes 1572896 | tf_op jit(solution)/shard_map/all_to_all | solution.py:40
  192.3 2.1 convert_bitcast_fusion
  194.4 2.4 %copy.25 = f32[1,384,4,512]{1,3,2,0:T(8,128)S(1)} copy(f32[1,384,4,512]{3,1,0,2:T(8,128)} %convert_bitcast_fusion) | data formatting | bytes 6291456 | tf_op jit(solution)/shard_map/convert_element_type | solution.py:42
  196.7 3.8 %fusion.12 = bf16[1,384,2048]{1,2,0:T(8,128)(2,1)} fusion(bf16[1,384,2048]{1,2,0:T(8,128)(2,1)} %copy.19, f32[1,384,4,512]{1,3,2,0:T(8,128)S(1)} %copy.25), kind=kLoop, calls=%fused_computation.22 | loop fusion | flops 8650752 | bytes 6291456 | tf_op jit(solution)/shard_map/convert_element_type | solution.py:43
  200.5 2.6 %copy.26 = bf16[1,384,2048]{2,1,0:T(8,128)(2,1)} copy(bf16[1,384,2048]{1,2,0:T(8,128)(2,1)} %fusion.12) | data formatting | bytes 3145728 | tf_op jit(solution)/shard_map/convert_element_type | solution.py:43
  (5 shorter events, 0.0 us)
Async XLA Ops:
  6.5 1.4 copy-start
  6.5 2.3 %copy-start.4 = (bf16[2048]{0:T(1024)(128)(2,1)S(1)}, bf16[2048]{0:T(1024)(128)(2,1)}, u32[]{:S(2)}) copy-start(bf16[2048]{0:T(1024)(128)(2,1)} %param.8) | copy-start | bytes 12292
  6.5 2.3 %copy-start.5 = (bf16[2048]{0:T(1024)(128)(2,1)S(1)}, bf16[2048]{0:T(1024)(128)(2,1)}, u32[]{:S(2)}) copy-start(bf16[2048]{0:T(1024)(128)(2,1)} %param.9) | copy-start | bytes 12292
  6.5 129.4 %all-gather.2.cloned.1.call-start = ((), (), s32[]{:S(2)}) async-start(), calls=%async_computation.2 | async-start | bytes 10485760 | tf_op jit(solution)/shard_map/all_gather | solution.py:16
  78.0 11.4 %copy-start.3 = (bf16[4,1024]{1,0:T(4,128)(2,1)S(1)}, bf16[4,1024]{1,0:T(4,128)(2,1)}, u32[]{:S(2)}) copy-start(bf16[4,1024]{1,0:T(4,128)(2,1)} %param.11) | copy-start | bytes 24580
  81.7 43.4 %all-to-all-start = ((bf16[4,2,98304]{2,1,0:T(2,128)(2,1)}), bf16[4,2,98304]{2,1,0:T(2,128)(2,1)}, u32[]{:S(2)}, u32[]{:S(2)}) async-start(bf16[4,2,98304]{2,1,0:T(2,128)(2,1)} %reshape.68), calls=%async_computation | async-start | bytes 3145728 | tf_op jit(solution)/shard_map/all_to_all | solution.py:37
  132.2 3.7 %copy-start.2 = (pred[1024,1024]{1,0:T(8,128)(4,1)S(1)}, pred[1024,1024]{1,0:T(8,128)(4,1)}, u32[]{:S(2)}) copy-start(pred[1024,1024]{1,0:T(8,128)(4,1)} %iota_compare_fusion) | copy-start | bytes 3145732
  150.8 4.9 %copy-start.1 = (bf16[1,384,2048]{2,1,0:T(8,128)(2,1)S(1)}, bf16[1,384,2048]{2,1,0:T(8,128)(2,1)}, u32[]{:S(2)}) copy-start(bf16[1,384,2048]{2,1,0:T(8,128)(2,1)} %param.6) | copy-start | bytes 4718596
  152.2 40.1 %all-to-all-start.1 = ((bf16[4,1,384,512]{3,2,1,0:T(8,128)(2,1)}), bf16[4,1,384,512]{3,2,1,0:T(8,128)(2,1)S(1)}, u32[]{:S(2)}, u32[]{:S(2)}) async-start(bf16[4,1,384,512]{3,2,1,0:T(8,128)(2,1)} %pad_maximum_fusion), calls=%async_computation.1 | async-start | bytes 3145728 | tf_op jit(solution)/shard_map/all_to_all | solution.py:40
Sparse Core Ops, SparseCore 0:
  8.9 60.9 all-gather.1
